TPU v7x, 32 devices: a whole 2x2x4 slice. The times are simulated.
32 devices in a mesh: sp: 8 (over z, y), tp: 4 (over x, core).
Axes of the slice: x: 2, y: 2, z: 4, core: 2. Of those that a mesh axis runs over, the one named last changes fastest.
Arguments:
- tokens: bfloat16 [2048, 4096], P(('sp', 'tp')), may hold values from -6 to 6, as said below
- query_one: bfloat16 [4096, 1024], P('sp', 'tp'), may hold values from -0.125 to 0.125
- query_two: bfloat16 [4096, 1024], P('sp', 'tp'), may hold values from -0.125 to 0.125
- key_one: bfloat16 [4096, 1024], P('sp', 'tp'), may hold values from -0.125 to 0.125
- key_two: bfloat16 [4096, 1024], P('sp', 'tp'), may hold values from -0.125 to 0.125
- value_weight: bfloat16 [4096, 2048], P('sp', 'tp'), may hold values from -0.09375 to 0.09375
- out_weight: bfloat16 [2048, 4096], P('tp', 'sp'), may hold values from -0.125 to 0.125
- lambdas: float32 [8], P('tp'), may hold values from 0.3 to 0.8
- head_gain: float32 [256], replicated, may hold values from 0.1 to 1.9
Outputs:
- layer_out: bfloat16 [2048, 4096], P(('sp', 'tp'))
Inputs may be any that keep to these rules, and one draw needn't show every extreme that they name: `tokens`: the features' mean changes between 16 equal spans of the sequence.
All inputs are finite; a program needn't handle non-finite values.
Results may differ from a plain program's by a relative error of at most 0.013.
The roundings to bfloat16 on the way count: a program that leaves them out, or rounds other values in their place, can miss the bound.
Values may be sent and summed in bfloat16 or wider, within the bound.
No kernel may reach another device: no remote copies, remote signals or barrier semaphores. Data moves between devices by JAX's collectives and lax.ppermute only.
A program may use at most 128 MiB of HBM per device.

v0:
```python
import jax
import jax.numpy as jnp
from jax import lax
from jax.sharding import PartitionSpec as P

QK = 128
V = 256
ROPE_BASE = 500000.0
EPS_NORM = 0.02


def rotate(values, positions):
    half_dim = values.shape[-1] // 2
    inverse = 1.0 / ROPE_BASE ** (
        jnp.arange(0, 2 * half_dim, 2, dtype=jnp.float32) / (2 * half_dim)
    )
    angles = positions.astype(jnp.float32)[:, None] * inverse[None, :]
    cos_part = jnp.cos(angles)[:, None, :]
    sin_part = jnp.sin(angles)[:, None, :]
    first_half = values[..., :half_dim]
    second_half = values[..., half_dim:]
    return jnp.concatenate(
        [
            first_half * cos_part - second_half * sin_part,
            second_half * cos_part + first_half * sin_part,
        ],
        axis=-1,
    )


def unchanged(carried):
    return carried


def on_device(
    tokens, query_one, query_two, key_one, key_two, value_weight, out_weight, lambdas, head_gain
):
    tp_count = lax.axis_size("tp")
    sp_index = lax.axis_index("sp")
    own_rows = tokens.shape[0]
    local_len = own_rows * tp_count
    half_len = local_len // 2
    heads_here = lambdas.shape[0]
    gathered = lax.all_gather(tokens, "tp", axis=0, tiled=True)
    row_ids = jnp.arange(local_len, dtype=jnp.int32)
    query_pos = sp_index * local_len + row_ids
    pieces = (
        lax.all_gather(query_one, "sp", axis=0, tiled=True),
        lax.all_gather(query_two, "sp", axis=0, tiled=True),
        lax.all_gather(key_one, "sp", axis=0, tiled=True),
        lax.all_gather(key_two, "sp", axis=0, tiled=True),
        lax.all_gather(value_weight, "sp", axis=0, tiled=True),
    )
    projected = tuple(
        (
            jnp.dot(gathered, weight_piece, preferred_element_type=jnp.float32)
            for weight_piece in pieces
        )
    )

    def turned(product):
        return rotate(product.reshape(local_len, heads_here, QK), query_pos).astype(jnp.bfloat16)

    q_one = turned(projected[0])
    q_two = turned(projected[1])
    k_one = turned(projected[2]).reshape(local_len, heads_here * QK)
    k_two = turned(projected[3]).reshape(local_len, heads_here * QK)
    values = projected[4].astype(jnp.bfloat16)
    scale = QK ** (-0.5)
    pieces = (
        lax.all_gather(k_one, "sp", axis=0, tiled=True),
        lax.all_gather(k_two, "sp", axis=0, tiled=True),
        lax.all_gather(values, "sp", axis=0, tiled=True),
    )
    key_count = pieces[0].shape[0]
    global_ids = jnp.arange(key_count, dtype=jnp.int32)
    shard_ids = global_ids // local_len
    within = global_ids % local_len
    key_pos = shard_ids * local_len + within
    key_sets = (
        pieces[0].reshape(key_count, heads_here, QK),
        pieces[1].reshape(key_count, heads_here, QK),
    )
    value_rows = pieces[2].reshape(key_count, heads_here, V)
    row_tops = jnp.full((2, heads_here, local_len), -1e30, jnp.float32)
    totals = jnp.zeros((2, heads_here, local_len), jnp.float32)
    accums = jnp.zeros((2, heads_here, local_len, V), jnp.float32)
    new_parts = []
    for segment in range(2):
        low_row = segment * half_len
        seg_pos = query_pos[low_row : low_row + half_len]
        queries = (q_one[low_row : low_row + half_len], q_two[low_row : low_row + half_len])
        carried = (
            row_tops[:, :, low_row : low_row + half_len],
            totals[:, :, low_row : low_row + half_len],
            accums[:, :, low_row : low_row + half_len],
        )

        def update(carried, queries=queries, seg_pos=seg_pos):
            allowed = key_pos[None, :] <= seg_pos[:, None]
            out_tops, out_totals, out_accums = ([], [], [])
            for map_index in range(2):
                scores = (
                    jnp.einsum(
                        "qhd,khd->hqk",
                        queries[map_index],
                        key_sets[map_index],
                        preferred_element_type=jnp.float32,
                    )
                    * scale
                )
                masked = jnp.where(allowed[None], scores, -1e30)
                old_top = carried[0][map_index]
                new_top = jnp.maximum(old_top, jnp.max(masked, axis=-1))
                exp_weights = jnp.where(allowed[None], jnp.exp(scores - new_top[..., None]), 0.0)
                new_total = jnp.sum(exp_weights, axis=-1)
                new_accum = jnp.einsum(
                    "hqk,khv->hqv",
                    exp_weights.astype(jnp.bfloat16),
                    value_rows,
                    preferred_element_type=jnp.float32,
                )
                out_tops.append(new_top)
                out_totals.append(new_total)
                out_accums.append(new_accum)
            return (jnp.stack(out_tops), jnp.stack(out_totals), jnp.stack(out_accums))

        needed = jnp.min(key_pos) <= jnp.max(seg_pos)
        new_parts.append(lax.cond(needed, update, unchanged, carried))
    row_tops, totals, accums = tuple(
        (
            jnp.concatenate([new_part[member] for new_part in new_parts], axis=2)
            for member in range(3)
        )
    )
    map_outputs = accums / totals[..., None]
    mixed_out = map_outputs[0] - lambdas[:, None, None] * map_outputs[1]
    scaled = (
        mixed_out
        * lax.rsqrt(jnp.mean(mixed_out * mixed_out, axis=-1, keepdims=True) + EPS_NORM)
        * head_gain
    )
    attended = scaled.astype(jnp.bfloat16)
    weight_piece = lax.all_gather(out_weight, "sp", axis=1, tiled=True)
    shaped = weight_piece.reshape(heads_here, V, weight_piece.shape[1])
    partial_terms = jnp.einsum("hqv,hvd->qd", attended, shaped, preferred_element_type=jnp.float32)
    summed = lax.psum_scatter(
        partial_terms.astype(jnp.bfloat16), "tp", scatter_dimension=0, tiled=True
    )
    return summed


def solution(mesh):
    in_specs = (
        P(("sp", "tp"), None),
        P("sp", "tp"),
        P("sp", "tp"),
        P("sp", "tp"),
        P("sp", "tp"),
        P("sp", "tp"),
        P("tp", "sp"),
        P("tp"),
        P(),
    )
    out_specs = P(("sp", "tp"), None)
    return jax.shard_map(
        on_device, mesh=mesh, in_specs=in_specs, out_specs=out_specs, check_vma=False
    )
```

profile of v0, /device:TPU:0, one launch (start us, length us, event | category | flops | bytes accessed | tf_op | source)
XLA Modules:
  0.0 554.6 jit_solution(14938328671323246360)
XLA Ops:
  10.5 23.7 %all-gather.11.cloned.1.call-done = bf16[256,4096]{1,0:T(8,128)(2,1)} async-done(((bf16[64,4096]{1,0:T(8,128)(2,1)}), bf16[256,4096]{1,0:T(8,128)(2,1)}) %all-gather.11.cloned.1.call-update) | async-done | bytes 2097168 | tf_op jit(solution)/shard_map/all_gather | solution.py:44
  34.2 74.9 %all-gather.25.cloned.1.call-done = bf16[4096,512]{1,0:T(8,128)(2,1)} async-done(((bf16[512,512]{1,0:T(8,128)(2,1)}), bf16[4096,512]{1,0:T(8,128)(2,1)}) %all-gather.25.cloned.1.call-update) | async-done | bytes 4194320 | tf_op jit(solution)/shard_map/all_gather | solution.py:52
  109.2 4.8 convolution_convert_fusion
  114.3 44.6 %all-gather.19.cloned.1.call-done = bf16[4096,256]{1,0:T(8,128)(2,1)} async-done(((bf16[512,256]{1,0:T(8,128)(2,1)}), bf16[4096,256]{1,0:T(8,128)(2,1)}) %all-gather.19.cloned.1.call-update) | async-done | bytes 2097168 | tf_op jit(solution)/shard_map/all_gather | solution.py:49
  159.0 2.5 fusion.74
  161.5 47.1 %all-gather.21.cloned.1.call-done = bf16[4096,256]{1,0:T(8,128)(2,1)} async-done(((bf16[512,256]{1,0:T(8,128)(2,1)}), bf16[4096,256]{1,0:T(8,128)(2,1)}) %all-gather.21.cloned.1.call-update) | async-done | bytes 2097168 | tf_op jit(solution)/shard_map/all_gather | solution.py:51
  208.6 2.5 fusion.75
  211.1 47.1 %all-gather.13.cloned.1.call-done = bf16[4096,256]{1,0:T(8,128)(2,1)} async-done(((bf16[512,256]{1,0:T(8,128)(2,1)}), bf16[4096,256]{1,0:T(8,128)(2,1)}) %all-gather.13.cloned.1.call-update) | async-done | bytes 2097168 | tf_op jit(solution)/shard_map/all_gather | solution.py:48
  258.2 2.5 fusion.72
  260.7 47.1 %all-gather.15.cloned.1.call-done = bf16[4096,256]{1,0:T(8,128)(2,1)} async-done(((bf16[512,256]{1,0:T(8,128)(2,1)}), bf16[4096,256]{1,0:T(8,128)(2,1)}) %all-gather.15.cloned.1.call-update) | async-done | bytes 2097168 | tf_op jit(solution)/shard_map/all_gather | solution.py:50
  307.8 2.5 fusion.73
  316.8 40.8 %all-gather.27.cloned.1.call-done = bf16[2048,512]{1,0:T(8,128)(2,1)} async-done(((bf16[256,512]{1,0:T(8,128)(2,1)}), bf16[2048,512]{1,0:T(8,128)(2,1)}) %all-gather.27.cloned.1.call-update) | async-done | bytes 2097168 | tf_op jit(solution)/shard_map/all_gather | solution.py:73
  357.6 4.0 reshape.172
  361.6 36.0 %all-gather.23.cloned.1.call-done = bf16[2048,256]{0,1:T(8,128)(2,1)} async-done(((bf16[256,256]{0,1:T(8,128)(2,1)}), bf16[2048,256]{0,1:T(8,128)(2,1)}) %all-gather.23.cloned.1.call-update) | async-done | bytes 1048592 | tf_op jit(solution)/shard_map/all_gather | solution.py:72
  397.6 40.5 %all-gather.17.cloned.1.call-done = bf16[2048,256]{0,1:T(8,128)(2,1)} async-done(((bf16[256,256]{0,1:T(8,128)(2,1)}), bf16[2048,256]{0,1:T(8,128)(2,1)}) %all-gather.17.cloned.1.call-update) | async-done | bytes 1048592 | tf_op jit(solution)/shard_map/all_gather | solution.py:71
  438.1 8.6 %conditional.2 = (f32[2,2,128]{2,1,0:T(2,128)S(1)}, f32[2,2,128,256]{3,2,1,0:T(8,128)}) conditional(s32[]{:T(128)} %convert_element_type.52, () %tuple.21, (s32[2048]{0:T(1024)S(1)}, s32[128]{0:T(128)S(1)}, bf16[256,2,128]{0,2,1:T(8,128)(2,1)S(1)}, bf16[2048,2,128]{0,2,1:T(8,128)(2,1)}, bf16[256,2,128]{0,2,1:T(8,128)(2,1)S(1)}, ...), branch_computations={%region_2.3_spmd, %region_3.8_spmd} | conditional | flops 815136768 | bytes 35283528 | solution.py:129
  439.1 1.9 select_reduce_fusion.1
  441.8 2.1 fusion.5
  446.7 10.4 %conditional.3 = (f32[2,2,128]{2,1,0:T(2,128)S(1)}, f32[2,2,128,256]{3,2,1,0:T(8,128)}) conditional(s32[]{:T(128)} %convert_element_type.57, () %tuple.23, (s32[2048]{0:T(1024)S(1)}, s32[128]{0:T(128)}, bf16[256,2,128]{0,2,1:T(8,128)(2,1)}, bf16[2048,2,128]{0,2,1:T(8,128)(2,1)}, bf16[256,2,128]{0,2,1:T(8,128)(2,1)S(1)}, ...), branch_computations={%region_9.10_spmd, %region_10.15_spmd} | conditional | flops 815136768 | bytes 35283528 | solution.py:129
  449.5 1.9 select_reduce_fusion.3
  452.2 2.1 fusion.31
  458.8 54.9 %all-gather.29.cloned.1.call-done = bf16[512,4096]{1,0:T(8,128)(2,1)} async-done(((bf16[512,512]{1,0:T(8,128)(2,1)}), bf16[512,4096]{1,0:T(8,128)(2,1)}) %all-gather.29.cloned.1.call-update) | async-done | bytes 4194320 | tf_op jit(solution)/shard_map/all_gather | solution.py:144
  513.7 4.8 fusion.52
  518.5 29.5 %reduce-scatter.2.cloned.1.call-done = bf16[64,4096]{1,0:T(8,128)(2,1)} async-done(((bf16[256,4096]{1,0:T(8,128)(2,1)}), bf16[64,4096]{1,0:T(8,128)(2,1)}) %reduce-scatter.2.cloned.1.call-update) | async-done | bytes 524304 | tf_op jit(solution)/shard_map/reduce_scatter | solution.py:147
  (73 shorter events, 20.7 us)
Async XLA Ops:
  6.5 27.7 %all-gather.11.cloned.1.call-start = ((), (), s32[]{:S(2)}) async-start(), calls=%async_computation.1 | async-start | bytes 2621440 | tf_op jit(solution)/shard_map/all_gather | solution.py:44
  7.3 101.9 %all-gather.25.cloned.1.call-start = ((), (), s32[]{:S(2)}) async-start(), calls=%async_computation.8 | async-start | bytes 4718592 | tf_op jit(solution)/shard_map/all_gather | solution.py:52
  8.0 150.9 %all-gather.19.cloned.1.call-start = ((), (), s32[]{:S(2)}) async-start(), calls=%async_computation.5 | async-start | bytes 2359296 | tf_op jit(solution)/shard_map/all_gather | solution.py:49
  8.7 199.9 %all-gather.21.cloned.1.call-start = ((), (), s32[]{:S(2)}) async-start(), calls=%async_computation.6 | async-start | bytes 2359296 | tf_op jit(solution)/shard_map/all_gather | solution.py:51
  9.3 248.9 %all-gather.13.cloned.1.call-start = ((), (), s32[]{:S(2)}) async-start(), calls=%async_computation.2 | async-start | bytes 2359296 | tf_op jit(solution)/shard_map/all_gather | solution.py:48
  9.9 297.9 %all-gather.15.cloned.1.call-start = ((), (), s32[]{:S(2)}) async-start(), calls=%async_computation.3 | async-start | bytes 2359296 | tf_op jit(solution)/shard_map/all_gather | solution.py:50
  10.5 347.1 %all-gather.27.cloned.1.call-start = ((), (), s32[]{:S(2)}) async-start(), calls=%async_computation.9 | async-start | bytes 2359296 | tf_op jit(solution)/shard_map/all_gather | solution.py:73
  34.2 124.7 %copy-start = (bf16[256,4096]{1,0:T(8,128)(2,1)S(1)}, bf16[256,4096]{1,0:T(8,128)(2,1)}, u32[]{:S(2)}) copy-start(bf16[256,4096]{1,0:T(8,128)(2,1)} %all-gather.11.cloned.1.call-done) | copy-start | bytes 6291460
  114.0 283.7 %all-gather.23.cloned.1.call-start = ((), (), s32[]{:S(2)}) async-start(), calls=%async_computation.7 | async-start | bytes 1179648 | tf_op jit(solution)/shard_map/all_gather | solution.py:72
  311.2 126.9 %all-gather.17.cloned.1.call-start = ((), (), s32[]{:S(2)}) async-start(), calls=%async_computation.4 | async-start | bytes 1179648 | tf_op jit(solution)/shard_map/all_gather | solution.py:71
  312.0 201.7 %all-gather.29.cloned.1.call-start = ((), (), s32[]{:S(2)}) async-start(), calls=%async_computation.10 | async-start | bytes 4718592 | tf_op jit(solution)/shard_map/all_gather | solution.py:144
  312.5 235.5 %reduce-scatter.2.cloned.1.call-start = ((), (), s32[]{:S(2)}) async-start(), calls=%async_computation.11 | async-start | bytes 2621440 | tf_op jit(solution)/shard_map/reduce_scatter | solution.py:147
  316.8 121.3 %copy-start.5 = (bf16[256,2,128]{0,2,1:T(8,128)(2,1)}, bf16[256,2,128]{0,2,1:T(8,128)(2,1)S(1)}, u32[]{:S(2)}) copy-start(bf16[256,2,128]{0,2,1:T(8,128)(2,1)S(1)} %pad_maximum_fusion.4) | copy-start | bytes 393220
  438.1 3.7 copy-start.1
  441.8 2.1 copy-start.3
  446.9 5.3 copy-start.2
  452.2 2.1 copy-start.4
  457.1 1.5 copy-start.6
  457.1 56.6 %copy-start.7 = (f32[256]{0:T(256)S(1)}, f32[256]{0:T(256)}, u32[]{:S(2)}) copy-start(f32[256]{0:T(256)} %param.21) | copy-start | bytes 3076
Sparse Core Ops, SparseCore 0:
  8.9 25.2 all-gather.10
  36.3 72.7 all-gather.24
  111.3 47.6 all-gather.18
  160.9 47.6 all-gather.20
  210.6 47.5 all-gather.12
  260.2 47.6 all-gather.14
  310.0 47.6 all-gather.26
  359.7 37.9 all-gather.22
  399.7 38.3 all-gather.16
  440.0 73.6 all-gather.28
  518.7 29.3 reduce-scatter.1
where the time goes:
time: 555 us
  waiting for transfers between devices  490 us (88%)
  matrix products  30.4 us (5%)
  between operations  15.7 us (3%)
  other arithmetic  9.28 us (2%)
  local copies, waits for them, and re-layouts  7.99 us (1%)
    all_gather x1, waiting for transfers between devices, on_device(): lax.all_gather(value_weight, 'sp', axis=0, tiled=True)  74.9 us
    all_gather x1, waiting for transfers between devices, on_device(): weight_piece = lax.all_gather(out_weight, 'sp', axis=1, tiled=True)  54.9 us
    all_gather x1, waiting for transfers between devices, on_device(): lax.all_gather(key_two, 'sp', axis=0, tiled=True)  47.1 us
    all_gather x1, waiting for transfers between devices, on_device(): lax.all_gather(key_one, 'sp', axis=0, tiled=True)  47.1 us
    all_gather x1, waiting for transfers between devices, on_device(): lax.all_gather(query_one, 'sp', axis=0, tiled=True)  47.1 us
    all_gather x1, waiting for transfers between devices, on_device(): lax.all_gather(query_two, 'sp', axis=0, tiled=True)  44.6 us
    all_gather x1, waiting for transfers between devices, on_device(): lax.all_gather(values, 'sp', axis=0, tiled=True)  40.8 us
    all_gather x1, waiting for transfers between devices, on_device(): lax.all_gather(k_one, 'sp', axis=0, tiled=True)  40.5 us
  transfers between devices with their start and end apart: 11, of which 11 were waited for; matrix products, arithmetic and copies ran while one was open for 8% of the time, Pallas kernels for 0%

commit v1 on v0

--- a/solution.py
+++ b/solution.py
@@ -7,6 +7,27 @@
 V = 256
 ROPE_BASE = 500000.0
 EPS_NORM = 0.02
+
+
+def joined_along(pieces, dim):
+    lengths = list(pieces.shape[1:])
+    lengths[dim] *= pieces.shape[0]
+    return jnp.moveaxis(pieces, 0, dim).reshape(lengths)
+
+
+def collected_by_bits(shard, axis):
+    size, position = (lax.axis_size(axis), lax.axis_index(axis))
+    pieces, bit = (shard[None], 1)
+    while bit < size:
+        other = lax.ppermute(pieces, axis, [(i, i ^ bit) for i in range(size)])
+        low = position & bit == 0
+        pieces = jnp.concatenate([jnp.where(low, pieces, other), jnp.where(low, other, pieces)])
+        bit *= 2
+    return pieces
+
+
+def doubled_up(x, axis, dim):
+    return joined_along(collected_by_bits(x, axis), dim)
 
 
 def rotate(values, positions):
@@ -47,7 +68,7 @@
     pieces = (
         lax.all_gather(query_one, "sp", axis=0, tiled=True),
         lax.all_gather(query_two, "sp", axis=0, tiled=True),
-        lax.all_gather(key_one, "sp", axis=0, tiled=True),
+        doubled_up(key_one, "sp", 0),
         lax.all_gather(key_two, "sp", axis=0, tiled=True),
         lax.all_gather(value_weight, "sp", axis=0, tiled=True),
     )

time: 555 us -> 546 us (0.984)
  waiting for transfers between devices: 490 us -> 472 us
  starting transfers between devices: 0.39 us -> 7.15 us
    ppermute x0 -> x3, waiting for transfers between devices: none -> 60 us  [collected_by_bits(): other = lax.ppermute(pieces, axis, [(i, i ^ bit) for i in range(size)])]
    all_gather x1 -> x0, waiting for transfers between devices: 47.1 us -> none  [on_device(): lax.all_gather(key_one, 'sp', axis=0, tiled=True)]
    all_gather x1, waiting for transfers between devices: 44.6 us -> 25.2 us  [on_device(): lax.all_gather(query_two, 'sp', axis=0, tiled=True)]
    all_gather x1, waiting for transfers between devices: 23.7 us -> 11.7 us  [on_device(): gathered = lax.all_gather(tokens, 'tp', axis=0, tiled=True)]
    ppermute x0 -> x3, starting transfers between devices: none -> 6.79 us  [collected_by_bits(): other = lax.ppermute(pieces, axis, [(i, i ^ bit) for i in range(size)])]
  transfers between devices with their start and end apart: 11 -> 13, of which waited for: 11 -> 12; matrix products, arithmetic and copies ran while one was open for 8% -> 8% of each run, Pallas kernels for 0% -> 0%
where the time goes in v1:
time: 546 us
  waiting for transfers between devices  472 us (86%)
  matrix products  28.7 us (5%)
  between operations  16.3 us (3%)
  other arithmetic  11.8 us (2%)
  local copies, waits for them, and re-layouts  9.4 us (2%)
  starting transfers between devices  7.15 us (1%)
    all_gather x1, waiting for transfers between devices, on_device(): lax.all_gather(value_weight, 'sp', axis=0, tiled=True)  75 us
    ppermute x3, waiting for transfers between devices, collected_by_bits(): other = lax.ppermute(pieces, axis, [(i, i ^ bit) for i in range(size)])  60 us
    all_gather x1, waiting for transfers between devices, on_device(): weight_piece = lax.all_gather(out_weight, 'sp', axis=1, tiled=True)  55.8 us
    all_gather x1, waiting for transfers between devices, on_device(): lax.all_gather(key_two, 'sp', axis=0, tiled=True)  47.1 us
    all_gather x1, waiting for transfers between devices, on_device(): lax.all_gather(query_one, 'sp', axis=0, tiled=True)  47.1 us
    all_gather x1, waiting for transfers between devices, on_device(): lax.all_gather(k_one, 'sp', axis=0, tiled=True)  40.5 us
    all_gather x1, waiting for transfers between devices, on_device(): lax.all_gather(values, 'sp', axis=0, tiled=True)  40.2 us
    all_gather x1, waiting for transfers between devices, on_device(): lax.all_gather(k_two, 'sp', axis=0, tiled=True)  36 us
  transfers between devices with their start and end apart: 13, of which 12 were waited for; matrix products, arithmetic and copies ran while one was open for 8% of the time, Pallas kernels for 0%

profile of v1, /device:TPU:0, one launch (start us, length us, event | category | flops | bytes accessed | tf_op | source)
XLA Modules:
  0.0 545.6 jit_solution(963950363977366892)
XLA Ops:
  10.0 3.1 collective-permute-start
  13.0 6.5 %collective-permute-done = bf16[1,512,256]{2,1,0:T(8,128)(2,1)S(1)} collective-permute-done((bf16[1,512,256]{2,1,0:T(8,128)(2,1)}, bf16[1,512,256]{2,1,0:T(8,128)(2,1)S(1)}, u32[]{:S(2)}, u32[]{:S(2)}) %collective-permute-start) | collective-permute-done | bytes 262176 | tf_op jit(solution)/shard_map/ppermute | solution.py:22
  22.5 11.7 %all-gather.10.cloned.1.call-done = bf16[256,4096]{1,0:T(8,128)(2,1)} async-done(((bf16[64,4096]{1,0:T(8,128)(2,1)}), bf16[256,4096]{1,0:T(8,128)(2,1)}) %all-gather.10.cloned.1.call-update) | async-done | bytes 2097168 | tf_op jit(solution)/shard_map/all_gather | solution.py:65
  34.2 75.0 %all-gather.22.cloned.1.call-done = bf16[4096,512]{1,0:T(8,128)(2,1)} async-done(((bf16[512,512]{1,0:T(8,128)(2,1)}), bf16[4096,512]{1,0:T(8,128)(2,1)}) %all-gather.22.cloned.1.call-update) | async-done | bytes 4194320 | tf_op jit(solution)/shard_map/all_gather | solution.py:73
  109.2 4.8 convolution_convert_fusion
  117.4 53.5 %collective-permute-done.2 = bf16[4,512,256]{2,1,0:T(8,128)(2,1)S(1)} collective-permute-done((bf16[4,512,256]{2,1,0:T(8,128)(2,1)}, bf16[4,512,256]{2,1,0:T(8,128)(2,1)S(1)}, u32[]{:S(2)}, u32[]{:S(2)}) %collective-permute-start.2) | collective-permute-done | bytes 1048608 | tf_op jit(solution)/shard_map/ppermute | solution.py:22
  173.4 25.2 %all-gather.16.cloned.1.call-done = bf16[4096,256]{1,0:T(8,128)(2,1)} async-done(((bf16[512,256]{1,0:T(8,128)(2,1)}), bf16[4096,256]{1,0:T(8,128)(2,1)}) %all-gather.16.cloned.1.call-update) | async-done | bytes 2097168 | tf_op jit(solution)/shard_map/all_gather | solution.py:70
  198.6 2.5 fusion.74
  201.1 47.1 %all-gather.18.cloned.1.call-done = bf16[4096,256]{1,0:T(8,128)(2,1)} async-done(((bf16[512,256]{1,0:T(8,128)(2,1)}), bf16[4096,256]{1,0:T(8,128)(2,1)}) %all-gather.18.cloned.1.call-update) | async-done | bytes 2097168 | tf_op jit(solution)/shard_map/all_gather | solution.py:72
  248.2 2.5 fusion.75
  250.8 47.1 %all-gather.12.cloned.1.call-done = bf16[4096,256]{1,0:T(8,128)(2,1)} async-done(((bf16[512,256]{1,0:T(8,128)(2,1)}), bf16[4096,256]{1,0:T(8,128)(2,1)}) %all-gather.12.cloned.1.call-update) | async-done | bytes 2097168 | tf_op jit(solution)/shard_map/all_gather | solution.py:69
  297.8 2.5 fusion.72
  307.3 40.2 %all-gather.24.cloned.1.call-done = bf16[2048,512]{1,0:T(8,128)(2,1)} async-done(((bf16[256,512]{1,0:T(8,128)(2,1)}), bf16[2048,512]{1,0:T(8,128)(2,1)}) %all-gather.24.cloned.1.call-update) | async-done | bytes 2097168 | tf_op jit(solution)/shard_map/all_gather | solution.py:94
  347.5 4.0 reshape.176
  351.5 36.0 %all-gather.20.cloned.1.call-done = bf16[2048,256]{0,1:T(8,128)(2,1)} async-done(((bf16[256,256]{0,1:T(8,128)(2,1)}), bf16[2048,256]{0,1:T(8,128)(2,1)}) %all-gather.20.cloned.1.call-update) | async-done | bytes 1048592 | tf_op jit(solution)/shard_map/all_gather | solution.py:93
  387.5 40.5 %all-gather.14.cloned.1.call-done = bf16[2048,256]{0,1:T(8,128)(2,1)} async-done(((bf16[256,256]{0,1:T(8,128)(2,1)}), bf16[2048,256]{0,1:T(8,128)(2,1)}) %all-gather.14.cloned.1.call-update) | async-done | bytes 1048592 | tf_op jit(solution)/shard_map/all_gather | solution.py:92
  428.0 8.6 %conditional.2 = (f32[2,2,128]{2,1,0:T(2,128)S(1)}, f32[2,2,128,256]{3,2,1,0:T(8,128)}) conditional(s32[]{:T(128)} %convert_element_type.52, () %tuple.21, (s32[2048]{0:T(1024)S(1)}, s32[128]{0:T(128)S(1)}, bf16[256,2,128]{0,2,1:T(8,128)(2,1)S(1)}, bf16[2048,2,128]{0,2,1:T(8,128)(2,1)}, bf16[256,2,128]{0,2,1:T(8,128)(2,1)S(1)}, ...), branch_computations={%region_2.3_spmd, %region_3.8_spmd} | conditional | flops 815136768 | bytes 35283528 | solution.py:150
  429.0 1.9 select_reduce_fusion.1
  431.7 2.1 fusion.5
  436.5 10.4 %conditional.3 = (f32[2,2,128]{2,1,0:T(2,128)S(1)}, f32[2,2,128,256]{3,2,1,0:T(8,128)}) conditional(s32[]{:T(128)} %convert_element_type.57, () %tuple.23, (s32[2048]{0:T(1024)S(1)}, s32[128]{0:T(128)}, bf16[256,2,128]{0,2,1:T(8,128)(2,1)}, bf16[2048,2,128]{0,2,1:T(8,128)(2,1)}, bf16[256,2,128]{0,2,1:T(8,128)(2,1)S(1)}, ...), branch_computations={%region_9.10_spmd, %region_10.15_spmd} | conditional | flops 815136768 | bytes 35283528 | solution.py:150
  442.0 2.1 fusion.31
  448.6 55.8 %all-gather.26.cloned.1.call-done = bf16[512,4096]{1,0:T(8,128)(2,1)} async-done(((bf16[512,512]{1,0:T(8,128)(2,1)}), bf16[512,4096]{1,0:T(8,128)(2,1)}) %all-gather.26.cloned.1.call-update) | async-done | bytes 4194320 | tf_op jit(solution)/shard_map/all_gather | solution.py:165
  504.5 4.8 fusion.52
  509.3 29.5 %reduce-scatter.2.cloned.1.call-done = bf16[64,4096]{1,0:T(8,128)(2,1)} async-done(((bf16[256,4096]{1,0:T(8,128)(2,1)}), bf16[64,4096]{1,0:T(8,128)(2,1)}) %reduce-scatter.2.cloned.1.call-update) | async-done | bytes 524304 | tf_op jit(solution)/shard_map/reduce_scatter | solution.py:168
  (82 shorter events, 30.7 us)
Async XLA Ops:
  6.5 27.7 %all-gather.10.cloned.1.call-start = ((), (), s32[]{:S(2)}) async-start(), calls=%async_computation.1 | async-start | bytes 2621440 | tf_op jit(solution)/shard_map/all_gather | solution.py:65
  7.3 101.9 %all-gather.22.cloned.1.call-start = ((), (), s32[]{:S(2)}) async-start(), calls=%async_computation.7 | async-start | bytes 4718592 | tf_op jit(solution)/shard_map/all_gather | solution.py:73
  8.0 190.6 %all-gather.16.cloned.1.call-start = ((), (), s32[]{:S(2)}) async-start(), calls=%async_computation.4 | async-start | bytes 2359296 | tf_op jit(solution)/shard_map/all_gather | solution.py:70
  8.7 239.5 %all-gather.18.cloned.1.call-start = ((), (), s32[]{:S(2)}) async-start(), calls=%async_computation.5 | async-start | bytes 2359296 | tf_op jit(solution)/shard_map/all_gather | solution.py:72
  9.3 288.5 %all-gather.12.cloned.1.call-start = ((), (), s32[]{:S(2)}) async-start(), calls=%async_computation.2 | async-start | bytes 2359296 | tf_op jit(solution)/shard_map/all_gather | solution.py:69
  9.9 337.6 %all-gather.24.cloned.1.call-start = ((), (), s32[]{:S(2)}) async-start(), calls=%async_computation.8 | async-start | bytes 2359296 | tf_op jit(solution)/shard_map/all_gather | solution.py:94
  10.0 9.6 %collective-permute-start = (bf16[1,512,256]{2,1,0:T(8,128)(2,1)}, bf16[1,512,256]{2,1,0:T(8,128)(2,1)S(1)}, u32[]{:S(2)}, u32[]{:S(2)}) collective-permute-start(bf16[1,512,256]{2,1,0:T(8,128)(2,1)} %bitcast.70), channel_id=1, source_target_pairs={{0,4},{4,0},{8,12},{12,8},{16,20},{20,16},{24,28},{28,24},{1,5},{5... | collective-permute-start | bytes 786440 | tf_op jit(solution)/shard_map/ppermute | solution.py:22
  20.6 93.4 %collective-permute-start.1 = (bf16[2,512,256]{2,1,0:T(8,128)(2,1)S(1)}, bf16[2,512,256]{2,1,0:T(8,128)(2,1)S(1)}, u32[]{:S(2)}, u32[]{:S(2)}) collective-permute-start(bf16[2,512,256]{2,1,0:T(8,128)(2,1)S(1)} %pad_maximum_fusion.6), channel_id=1, source_target_pairs={{0,8},{4,12},{8,0},{12,4},{16,24},{20,28},{24,16},{28,20},{1,9},{5... | collective-permute-start | bytes 1572872 | tf_op jit(solution)/shard_map/ppermute | solution.py:22
  114.0 273.5 %all-gather.20.cloned.1.call-start = ((), (), s32[]{:S(2)}) async-start(), calls=%async_computation.6 | async-start | bytes 1179648 | tf_op jit(solution)/shard_map/all_gather | solution.py:93
  115.2 55.7 %collective-permute-start.2 = (bf16[4,512,256]{2,1,0:T(8,128)(2,1)}, bf16[4,512,256]{2,1,0:T(8,128)(2,1)S(1)}, u32[]{:S(2)}, u32[]{:S(2)}) collective-permute-start(bf16[4,512,256]{2,1,0:T(8,128)(2,1)} %pad_maximum_fusion.5), channel_id=1, source_target_pairs={{0,16},{4,20},{8,24},{12,28},{16,0},{20,4},{24,8},{28,12},{1,17},{... | collective-permute-start | bytes 3145736 | tf_op jit(solution)/shard_map/ppermute | solution.py:22
  171.0 1.6 copy-start
  301.2 126.7 %all-gather.14.cloned.1.call-start = ((), (), s32[]{:S(2)}) async-start(), calls=%async_computation.3 | async-start | bytes 1179648 | tf_op jit(solution)/shard_map/all_gather | solution.py:92
  302.0 202.5 %all-gather.26.cloned.1.call-start = ((), (), s32[]{:S(2)}) async-start(), calls=%async_computation.9 | async-start | bytes 4718592 | tf_op jit(solution)/shard_map/all_gather | solution.py:165
  302.7 236.1 %reduce-scatter.2.cloned.1.call-start = ((), (), s32[]{:S(2)}) async-start(), calls=%async_computation.10 | async-start | bytes 2621440 | tf_op jit(solution)/shard_map/reduce_scatter | solution.py:168
  307.3 120.7 %copy-start.5 = (bf16[256,2,128]{0,2,1:T(8,128)(2,1)}, bf16[256,2,128]{0,2,1:T(8,128)(2,1)S(1)}, u32[]{:S(2)}) copy-start(bf16[256,2,128]{0,2,1:T(8,128)(2,1)S(1)} %pad_maximum_fusion.7) | copy-start | bytes 393220
  428.0 3.7 copy-start.1
  431.7 2.1 copy-start.3
  436.7 5.3 copy-start.2
  442.0 2.1 copy-start.4
  446.9 1.5 copy-start.6
  446.9 57.5 %copy-start.7 = (f32[256]{0:T(256)S(1)}, f32[256]{0:T(256)}, u32[]{:S(2)}) copy-start(f32[256]{0:T(256)} %param.21) | copy-start | bytes 3076
Sparse Core Ops, SparseCore 0:
  8.9 25.2 all-gather.9
  36.3 72.7 all-gather.21
  111.3 87.2 all-gather.15
  200.6 47.6 all-gather.17
  250.2 47.5 all-gather.11
  299.8 47.6 all-gather.23
  349.5 37.9 all-gather.19
  389.5 38.3 all-gather.13
  430.0 74.3 all-gather.25
  509.4 29.3 reduce-scatter.1
